TPU v7x, 32 devices: a whole 2x2x4 slice. The times are simulated.
32 devices in a mesh: ep: 4 (over y, x), tp: 8 (over z, core).
Axes of the slice: x: 2, y: 2, z: 4, core: 2. Of those that a mesh axis runs over, the one named last changes fastest.
Arguments:
- hidden: bfloat16 [160, 4096], P('ep', 'tp'), may hold values from -6 to 6
- positions: int32 [160], P('ep'), may hold values from 0 to 16383
- ret_state: float32 [160, 16, 128, 128], P('ep', 'tp'), may hold values from -1.5 to 1.5
- query_weight: bfloat16 [4096, 2048], P('ep', 'tp'), may hold values from -0.09375 to 0.09375
- key_weight: bfloat16 [4096, 2048], P('ep', 'tp'), may hold values from -0.09375 to 0.09375
- value_weight: bfloat16 [4096, 2048], P('ep', 'tp'), may hold values from -0.09375 to 0.09375
- gate_weight: bfloat16 [4096, 2048], P('ep', 'tp'), may hold values from -0.09375 to 0.09375
- head_gain: float32 [2048], P('tp'), may hold values from 0.1 to 1.9
- out_weight: bfloat16 [2048, 4096], P(None, 'tp'), may hold values from -0.125 to 0.125
- mix_gain: float32 [4096], replicated, may hold values from 0.1 to 1.9
- ffn_gain: float32 [4096], replicated, may hold values from 0.1 to 1.9
- expert_gate: bfloat16 [8, 4096, 2048], P('ep', None, 'tp'), may hold values from -0.09375 to 0.09375
- expert_up: bfloat16 [8, 4096, 2048], P('ep', None, 'tp'), may hold values from -0.09375 to 0.09375
- expert_down: bfloat16 [8, 2048, 4096], P('ep', None, 'tp'), may hold values from -0.125 to 0.125
- route_ids: int32 [160, 2], P('ep'), may hold values from 0 to 7, as said below
- route_weight: float32 [160, 2], P('ep'), may hold values from 0.25 to 1
Outputs:
- updated: bfloat16 [160, 4096], P('ep', 'tp')
- next_state: float32 [160, 16, 128, 128], P('ep', 'tp')
Inputs may be any that keep to these rules, and one draw needn't show every extreme that they name: `route_ids`: each row names two different experts of one group, the group being the numbers g * 2 to g * 2 + 1; in the rows of one device (aligned blocks of 40 rows) no expert is named more than 10 times, and some expert is named exactly 10 times.
All inputs are finite; a program needn't handle non-finite values.
Results may differ from a plain program's by a relative error of at most 0.014.
Values may be sent and summed in bfloat16 or wider, within the bound.
A program may use at most 64 MiB of HBM per device.

v0:
```python
import jax
import jax.numpy as jnp
from jax import lax
from jax.sharding import PartitionSpec as P

D = 4096
HEADS = 16
HEAD = 128
GROUPS = 4
TOP = 2
epsilon = 1e-06
rope_base = 10000.0


def rms_scale(rows, gain):
    values = rows.astype(jnp.float32)
    factor = lax.rsqrt(jnp.mean(values * values, axis=-1, keepdims=True) + epsilon)
    return (values * factor * gain).astype(jnp.bfloat16)


def log_decay(head_ids):
    return jnp.log(1.0 - 2.0 ** (-5.0 - 5.0 * head_ids.astype(jnp.float32) / (HEADS - 1)))


def rotate(values, positions):
    width = values.shape[-1]
    inverse = 1.0 / rope_base ** (jnp.arange(0, width, 2, dtype=jnp.float32) / width)
    angle = positions.astype(jnp.float32)[:, None, None] * inverse[None, None, :]
    cosine = jnp.cos(angle)
    sine = jnp.sin(angle)
    first = values[..., : width // 2]
    second = values[..., width // 2 :]
    return jnp.concatenate(
        [first * cosine - second * sine, first * sine + second * cosine], axis=-1
    )


def retain(query, key_rows, value_rows, gate_rows, ret_state, positions, head_ids, head_gain):
    batch = query.shape[0]
    heads = head_ids.shape[0]

    def split(array):
        return array.astype(jnp.float32).reshape(batch, heads, HEAD)

    rotated_query = rotate(split(query), positions)
    rotated_key = rotate(split(key_rows), positions) * HEAD ** (-0.5)
    value_heads = split(value_rows)
    decay = jnp.exp(log_decay(head_ids))
    next_state = (
        decay[None, :, None, None] * ret_state
        + rotated_key[..., :, None] * value_heads[..., None, :]
    )
    read = jnp.einsum("bhd,bhde->bhe", rotated_query, next_state, precision=lax.Precision.HIGHEST)
    centered = read - jnp.mean(read, axis=-1, keepdims=True)
    normal = centered * lax.rsqrt(jnp.mean(centered * centered, axis=-1, keepdims=True) + epsilon)
    mixed = (
        normal.reshape(batch, heads * HEAD) * head_gain * jax.nn.silu(gate_rows.astype(jnp.float32))
    )
    return (mixed.astype(jnp.bfloat16), next_state)


def per_device(
    hidden,
    positions,
    ret_state,
    query_weight,
    key_weight,
    value_weight,
    gate_weight,
    head_gain,
    out_weight,
    mix_gain,
    ffn_gain,
    expert_gate,
    expert_up,
    expert_down,
    route_ids,
    route_weight,
):
    own_rows = hidden.shape[0]
    slice_width = hidden.shape[1]
    full_rows = lax.all_gather(hidden, "tp", axis=1, tiled=True)
    normed = rms_scale(full_rows, mix_gain)
    columns = lax.all_to_all(normed, "ep", split_axis=1, concat_axis=0, tiled=True)
    stacked = jnp.concatenate([query_weight, key_weight, value_weight, gate_weight], axis=1)
    width = query_weight.shape[1]
    joined = lax.psum_scatter(
        jnp.dot(columns, stacked, preferred_element_type=jnp.float32),
        "ep",
        scatter_dimension=0,
        tiled=True,
    )
    sums = tuple((joined[:, number * width : (number + 1) * width] for number in range(4)))
    query, key_rows, value_rows, gate_rows = tuple((total.astype(jnp.bfloat16) for total in sums))
    heads_here = query_weight.shape[1] // HEAD
    head_ids = lax.axis_index("tp") * heads_here + jnp.arange(heads_here, dtype=jnp.int32)
    mixed, next_state = retain(
        query, key_rows, value_rows, gate_rows, ret_state, positions, head_ids, head_gain
    )
    projected = jnp.dot(
        lax.all_gather(mixed, "tp", axis=1, tiled=True),
        out_weight,
        preferred_element_type=jnp.float32,
    )
    after = (hidden.astype(jnp.float32) + projected).astype(jnp.bfloat16)
    local_experts = expert_gate.shape[0]
    peers = lax.axis_size("ep")
    experts = local_experts * peers
    group_size = experts // GROUPS
    capacity = 2 * ((own_rows // GROUPS + group_size - 1) // group_size)
    chosen = route_ids.reshape(-1)
    onehot = (chosen[:, None] == jnp.arange(experts, dtype=jnp.int32)[None, :]).astype(jnp.int32)
    ranks = jnp.sum((jnp.cumsum(onehot, axis=0) - 1) * onehot, axis=1)
    send_slot = chosen * capacity + ranks
    slot_count = experts * capacity
    placing = (jnp.arange(slot_count, dtype=jnp.int32)[:, None] == send_slot[None, :]).astype(
        jnp.float32
    )
    token_place = jnp.sum(placing.reshape(slot_count, own_rows, TOP), axis=2).astype(jnp.bfloat16)
    after_float = after.astype(jnp.float32)
    squares = lax.psum(jnp.sum(after_float * after_float, axis=1), "tp")
    gain_slice = lax.dynamic_slice_in_dim(
        ffn_gain, lax.axis_index("tp") * slice_width, slice_width, 0
    )
    factor = lax.rsqrt(squares / D + epsilon)
    scaled = (after_float * factor[:, None] * gain_slice).astype(jnp.bfloat16)
    packed = jnp.dot(token_place, scaled, preferred_element_type=jnp.float32).astype(jnp.bfloat16)
    arrived = lax.all_to_all(
        packed.reshape(peers, local_experts, capacity, scaled.shape[1]),
        "ep",
        split_axis=0,
        concat_axis=2,
        tiled=True,
    )
    arrived = lax.all_gather(arrived, "tp", axis=3, tiled=True)
    arrived = arrived.reshape(local_experts, peers * capacity, D)
    gate = jnp.einsum("emd,edf->emf", arrived, expert_gate, preferred_element_type=jnp.float32)
    lifted = jnp.einsum("emd,edf->emf", arrived, expert_up, preferred_element_type=jnp.float32)
    activated = (jax.nn.silu(gate) * lifted).astype(jnp.bfloat16)
    out_width = expert_down.shape[2]
    result = jnp.einsum(
        "emf,efd->emd",
        lax.all_gather(activated, "tp", axis=2, tiled=True),
        expert_down,
        preferred_element_type=jnp.float32,
    ).astype(jnp.bfloat16)
    back = lax.all_to_all(
        result.reshape(local_experts, peers, capacity, out_width),
        "ep",
        split_axis=1,
        concat_axis=1,
        tiled=True,
    )
    returned_rows = back.reshape(local_experts * peers * capacity, out_width)
    source_row = (
        chosen % local_experts * (peers * capacity) + chosen // local_experts * capacity + ranks
    )
    values = returned_rows[source_row].astype(jnp.float32).reshape(own_rows, TOP, out_width)
    weighted = jnp.sum(values * route_weight[:, :, None], axis=1)
    updated = (after.astype(jnp.float32) + weighted).astype(jnp.bfloat16)
    return (updated, next_state)


def solution(mesh):
    return jax.shard_map(
        per_device,
        mesh=mesh,
        in_specs=(
            P("ep", "tp"),
            P("ep"),
            P("ep", "tp", None, None),
            P("ep", "tp"),
            P("ep", "tp"),
            P("ep", "tp"),
            P("ep", "tp"),
            P("tp"),
            P(None, "tp"),
            P(),
            P(),
            P("ep", None, "tp"),
            P("ep", None, "tp"),
            P("ep", None, "tp"),
            P("ep", None),
            P("ep", None),
        ),
        out_specs=(P("ep", "tp"), P("ep", "tp", None, None)),
        check_vma=False,
    )
```

profile of v0, /device:TPU:0, one launch (start us, length us, event | category | flops | bytes accessed | tf_op | source)
XLA Modules:
  0.0 168.9 jit_solution(997779446454232462)
XLA Ops:
  7.2 0.0 copy-start
  7.2 0.0 reduce-scatter.4.cloned.1.call-start
  7.2 16.4 %all_gather.12 = bf16[40,4096]{1,0:T(8,128)(2,1)S(1)} all-gather(bf16[40,512]{1,0:T(8,128)(2,1)} %param.16), channel_id=1, replica_groups=mesh['ep'=4,'tp'=8] {'tp'}, dimensions={1}, use_global_device_ids=true | all-gather | bytes 368640 | tf_op jit(solution)/shard_map/all_gather | solution.py:82
  23.6 0.2 fusion.11
  23.8 0.9 fusion.13
  24.7 10.6 %all_to_all.42 = bf16[40,4,1024]{2,0,1:T(8,128)(2,1)S(1)} all-to-all(bf16[40,4,1024]{2,0,1:T(8,128)(2,1)S(1)} %bitcast.48), channel_id=1, replica_groups=mesh['ep'=4,'tp'=8] {'ep'}, dimensions={1} | all-to-all | bytes 655360 | tf_op jit(solution)/shard_map/all_to_all | solution.py:84
  35.3 0.0 copy-start.5
  35.3 0.0 copy-start.8
  35.3 2.9 %fusion = f32[160,1024]{1,0:T(8,128)} fusion(bf16[160,1024]{1,0:T(8,128)(2,1)S(1)} %bitcast.52, bf16[1024,256]{1,0:T(8,128)(2,1)} %param.22, bf16[1024,256]{1,0:T(8,128)(2,1)} %param.21, bf16[1024,256]{1,0:T(8,128)(2,1)} %param.20, bf16[1024,256]{1,0:T(8,128)(2,1)} %param.19), kind=kOutput, calls=%fused_computation.2 | convolution fusion | flops 343932928 | bytes 3080192 | tf_op jit(solution)/shard_map/dot_general | solution.py:88
  38.2 0.0 reduce-scatter.4.cloned.1.call-update
  38.3 0.0 copy-done.5
  38.3 0.1 copy.65
  38.4 0.1 eq.32
  38.5 0.1 reshape.300
  38.6 0.0 copy-done.8
  38.6 0.1 fusion.23
  38.7 0.1 reduce_window_sum.11
  38.8 0.2 select_reduce_fusion
  39.0 0.1 reduce_sum.71
  39.1 0.1 copy.66
  39.2 0.8 dynamic_slice.3
  40.0 0.1 convert_reduce_fusion
  40.1 0.2 multiply_cosine_fusion
  40.3 23.2 %reduce-scatter.4.cloned.1.call-done = f32[40,1024]{1,0:T(8,128)} async-done(((f32[160,1024]{1,0:T(8,128)}), f32[40,1024]{1,0:T(8,128)}) %reduce-scatter.4.cloned.1.call-update) | async-done | bytes 163856
  63.4 0.9 convert.10
  64.5 0.2 multiply_subtract_fusion
  64.7 0.2 pad_maximum_fusion
  64.9 4.0 %multiply_add_fusion = f32[40,2,128,128]{3,2,1,0:T(8,128)S(1)} fusion(f32[40,2,128,128]{3,2,1,0:T(8,128)} %param.18, f32[40,2,128]{2,1,0:T(2,128)S(1)} %reshape.305, f32[40,2,128]{2,1,0:T(2,128)S(1)} %get-tuple-element.16, f32[2]{0:T(128)S(1)} %log_exponential_fusion), kind=kLoop, calls=%fused_computation.1 | loop fusion | flops 3932160 | bytes 10567688 | tf_op jit(solution)/shard_map/add | solution.py:50
  68.9 0.0 copy-start.1
  68.9 0.0 copy-start.7
  68.9 0.0 copy-start.4
  68.9 2.3 %copy-done.1 = f32[40,2,128,128]{3,2,1,0:T(8,128)} copy-done((f32[40,2,128,128]{3,2,1,0:T(8,128)}, f32[40,2,128,128]{3,2,1,0:T(8,128)S(1)}, u32[]{:S(2)}) %copy-start.1) | copy-done | bytes 5242904
  71.3 0.0 copy-start.6
  71.3 4.5 %fusion.31 = f32[40,2,1,128]{3,2,1,0:T(1,128)S(1)} fusion(f32[40,2,128,1]{2,3,1,0:T(1,128)S(1)} %bitcast.55, f32[40,2,128,128]{3,2,1,0:T(8,128)S(1)} %multiply_add_fusion), kind=kOutput, calls=%fused_computation.78 | convolution fusion | flops 15728640 | bytes 5324800 | tf_op jit(solution)/shard_map/bhd,bhde->bhe/dot_general | solution.py:53
  75.8 0.1 reduce_sum.68
  76.0 0.2 multiply_reduce_fusion.2
  76.2 0.1 subtract_multiply_fusion
  76.3 0.0 copy-done.7
  76.4 14.2 %all_gather.13 = bf16[40,2048]{1,0:T(8,128)(2,1)S(1)} all-gather(bf16[40,256]{1,0:T(8,128)(2,1)S(1)} %fusion.24), channel_id=1, replica_groups=mesh['ep'=4,'tp'=8] {'tp'}, dimensions={1}, use_global_device_ids=true | all-gather | bytes 184320 | tf_op jit(solution)/shard_map/all_gather | solution.py:101
  90.5 0.0 copy-done
  90.5 0.0 copy-done.4
  90.5 0.6 multiply_reduce_fusion.1
  91.1 16.8 %psum.7 = f32[40]{0:T(128)S(1)} all-reduce(f32[40]{0:T(128)S(1)} %get-tuple-element.13), channel_id=1, replica_groups=mesh['ep'=4,'tp'=8] {'tp'}, use_global_device_ids=true, to_apply=%region_8.9 | all-reduce | flops 40 | bytes 320 | tf_op jit(solution)/shard_map/psum | solution.py:121
  107.9 0.2 convolution_convert_fusion.1
  108.2 0.7 copy.67
  108.9 3.3 %all-to-all-start.1 = ((bf16[4,2,10,512]{3,1,2,0:T(2,128)(2,1)}), bf16[4,2,10,512]{3,1,2,0:T(2,128)(2,1)S(1)}, u32[]{:S(2)}, u32[]{:S(2)}) async-start(bf16[4,2,10,512]{3,1,2,0:T(2,128)(2,1)} %copy.67), calls=%async_computation.1 | async-start | bytes 163840 | tf_op jit(solution)/shard_map/all_to_all | solution.py:128
  112.2 0.0 copy-done.6
  112.2 0.1 copy.72
  112.3 4.7 %all-to-all-done.1 = bf16[4,2,10,512]{3,1,2,0:T(2,128)(2,1)S(1)} async-done(((bf16[4,2,10,512]{3,1,2,0:T(2,128)(2,1)}), bf16[4,2,10,512]{3,1,2,0:T(2,128)(2,1)S(1)}, u32[]{:S(2)}, u32[]{:S(2)}) %all-to-all-start.1) | async-done | bytes 81952 | tf_op jit(solution)/shard_map/all_to_all | solution.py:128
  117.0 15.5 %all_gather.14 = bf16[1,2,40,4096]{3,2,1,0:T(8,128)(2,1)S(1)} all-gather(bf16[1,2,40,512]{3,2,1,0:T(8,128)(2,1)S(1)} %copy.68), channel_id=1, replica_groups=mesh['ep'=4,'tp'=8] {'tp'}, dimensions={3}, use_global_device_ids=true | all-gather | bytes 737280 | tf_op jit(solution)/shard_map/all_gather | solution.py:135
  132.5 2.9 %fusion.15 = f32[2,40,256]{2,1,0:T(8,128)S(1)} fusion(bf16[2,4096,256]{2,1,0:T(8,128)(2,1)} %param.27, bf16[1,2,40,4096]{3,2,1,0:T(8,128)(2,1)S(1)} %all_gather.14), kind=kOutput, calls=%fused_computation.23 | convolution fusion | flops 167772160 | bytes 4931584 | tf_op jit(solution)/shard_map/emd,edf->emf/dot_general | solution.py:137
  135.4 0.0 copy-done.3
  135.4 0.0 copy-start.2
  135.4 0.7 fusion.8
  136.1 14.4 %all_gather.15 = bf16[2,40,2048]{2,1,0:T(8,128)(2,1)S(1)} all-gather(bf16[2,40,256]{2,1,0:T(8,128)(2,1)S(1)} %fusion.8), channel_id=1, replica_groups=mesh['ep'=4,'tp'=8] {'tp'}, dimensions={2}, use_global_device_ids=true | all-gather | bytes 368640 | tf_op jit(solution)/shard_map/all_gather | solution.py:143
  150.5 0.0 copy-done.2
  150.5 0.8 convolution_convert_fusion
  151.3 0.7 copy.69
  152.0 3.3 %all-to-all-start.2 = ((bf16[2,4,10,512]{3,0,2,1:T(2,128)(2,1)}), bf16[2,4,10,512]{3,0,2,1:T(2,128)(2,1)S(1)}, u32[]{:S(2)}, u32[]{:S(2)}) async-start(bf16[2,4,10,512]{3,0,2,1:T(2,128)(2,1)} %bitcast.10), calls=%async_computation.2 | async-start | bytes 163840 | tf_op jit(solution)/shard_map/all_to_all | solution.py:147
  155.4 4.8 %all-to-all-done.2 = bf16[2,4,10,512]{3,0,2,1:T(2,128)(2,1)S(1)} async-done(((bf16[2,4,10,512]{3,0,2,1:T(2,128)(2,1)}), bf16[2,4,10,512]{3,0,2,1:T(2,128)(2,1)S(1)}, u32[]{:S(2)}, u32[]{:S(2)}) %all-to-all-start.2) | async-done | bytes 81952 | tf_op jit(solution)/shard_map/all_to_all | solution.py:147
  160.3 0.7 gather_fusion
  161.0 0.1 reshape.306
  161.1 0.3 multiply_reduce_fusion
  161.4 0.6 add_convert_fusion
  (21 shorter events, 0.3 us)
Async XLA Ops:
  7.2 83.4 %copy-start = (bf16[2048,512]{1,0:T(8,128)(2,1)S(1)}, bf16[2048,512]{1,0:T(8,128)(2,1)}, u32[]{:S(2)}) copy-start(bf16[2048,512]{1,0:T(8,128)(2,1)} %param.24) | copy-start | bytes 6291460
  7.2 56.3 %reduce-scatter.4.cloned.1.call-start = ((), (), s32[]{:S(2)}) async-start(), calls=%async_computation.4 | async-start | bytes 819200
  35.3 2.9 %copy-start.5 = (s32[40,2]{0,1:T(2,128)S(1)}, s32[40,2]{0,1:T(2,128)}, u32[]{:S(2)}) copy-start(s32[40,2]{0,1:T(2,128)} %param.30) | copy-start | bytes 964
  35.3 3.3 %copy-start.8 = (s32[40]{0:T(128)S(1)}, s32[40]{0:T(128)}, u32[]{:S(2)}) copy-start(s32[40]{0:T(128)} %param.17) | copy-start | bytes 484
  68.9 2.4 %copy-start.1 = (f32[40,2,128,128]{3,2,1,0:T(8,128)}, f32[40,2,128,128]{3,2,1,0:T(8,128)S(1)}, u32[]{:S(2)}) copy-start(f32[40,2,128,128]{3,2,1,0:T(8,128)S(1)} %multiply_add_fusion) | copy-start | bytes 15728644
  68.9 7.4 %copy-start.7 = (f32[256]{0:T(256)S(1)}, f32[256]{0:T(256)}, u32[]{:S(2)}) copy-start(f32[256]{0:T(256)} %param.23) | copy-start | bytes 3076
  68.9 21.6 %copy-start.4 = (bf16[40,512]{1,0:T(8,128)(2,1)S(1)}, bf16[40,512]{1,0:T(8,128)(2,1)}, u32[]{:S(2)}) copy-start(bf16[40,512]{1,0:T(8,128)(2,1)} %param.16) | copy-start | bytes 122884
  71.3 40.9 %copy-start.6 = (f32[40,2]{0,1:T(2,128)S(1)}, f32[40,2]{0,1:T(2,128)}, u32[]{:S(2)}) copy-start(f32[40,2]{0,1:T(2,128)} %param.31) | copy-start | bytes 964
  108.9 8.2 %all-to-all-start.1 = ((bf16[4,2,10,512]{3,1,2,0:T(2,128)(2,1)}), bf16[4,2,10,512]{3,1,2,0:T(2,128)(2,1)S(1)}, u32[]{:S(2)}, u32[]{:S(2)}) async-start(bf16[4,2,10,512]{3,1,2,0:T(2,128)(2,1)} %copy.67), calls=%async_computation.1 | async-start | bytes 163840 | tf_op jit(solution)/shard_map/all_to_all | solution.py:128
  117.0 18.4 %copy-start.3 = (bf16[2,4096,256]{2,1,0:T(8,128)(2,1)S(1)}, bf16[2,4096,256]{2,1,0:T(8,128)(2,1)}, u32[]{:S(2)}) copy-start(bf16[2,4096,256]{2,1,0:T(8,128)(2,1)} %param.28) | copy-start | bytes 12582916
  135.4 15.1 %copy-start.2 = (bf16[2,2048,512]{2,1,0:T(8,128)(2,1)S(1)}, bf16[2,2048,512]{2,1,0:T(8,128)(2,1)}, u32[]{:S(2)}) copy-start(bf16[2,2048,512]{2,1,0:T(8,128)(2,1)} %param.29) | copy-start | bytes 12582916
  152.0 8.2 %all-to-all-start.2 = ((bf16[2,4,10,512]{3,0,2,1:T(2,128)(2,1)}), bf16[2,4,10,512]{3,0,2,1:T(2,128)(2,1)S(1)}, u32[]{:S(2)}, u32[]{:S(2)}) async-start(bf16[2,4,10,512]{3,0,2,1:T(2,128)(2,1)} %bitcast.10), calls=%async_computation.2 | async-start | bytes 163840 | tf_op jit(solution)/shard_map/all_to_all | solution.py:147
Sparse Core Ops, SparseCore 0:
  38.4 25.0 reduce-scatter.3
where the time goes:
time: 169 us
  blocking collectives  87.8 us (52%)
  waiting for transfers between devices  32.8 us (19%)
  between operations  14.4 us (9%)
  matrix products  12.6 us (7%)
  other arithmetic  8.45 us (5%)
  starting transfers between devices  6.62 us (4%)
  local copies, waits for them, and re-layouts  6.2 us (4%)
    unnamed x2, waiting for transfers between devices  23.2 us
    psum x1, blocking collectives, per_device(): squares = lax.psum(jnp.sum(after_float * after_float, axis=1), 'tp')  16.8 us
    all_gather x1, blocking collectives, per_device(): full_rows = lax.all_gather(hidden, 'tp', axis=1, tiled=True)  16.4 us
    all_gather x1, blocking collectives, per_device(): arrived = lax.all_gather(arrived, 'tp', axis=3, tiled=True)  15.5 us
    all_gather x1, blocking collectives, per_device(): lax.all_gather(activated, 'tp', axis=2, tiled=True)  14.4 us
    all_gather x1, blocking collectives, per_device(): lax.all_gather(mixed, 'tp', axis=1, tiled=True)  14.2 us
    all_to_all x1, blocking collectives, per_device(): lax.all_to_all(normed, 'ep', split_axis=1, concat_axis=0, tiled=True)  10.6 us
    all_to_all x1, waiting for transfers between devices, per_device(): lax.all_to_all(result.reshape(local_experts, peers, capacity, out_width),...  4.84 us
  transfers between devices with their start and end apart: 3, of which 3 were waited for; matrix products, arithmetic and copies ran while one was open for 1% of the time, Pallas kernels for 0%

commit v1 on v0

--- a/solution.py
+++ b/solution.py
@@ -10,6 +10,18 @@
 TOP = 2
 epsilon = 1e-06
 rope_base = 10000.0
+
+
+def ring_product(value, axis, dim, product):
+    peers, position = (lax.axis_size(axis), lax.axis_index(axis))
+    left = [(i, (i - 1) % peers) for i in range(peers)]
+    rows = value.shape[dim]
+    current = value
+    so_far = product(current, position * rows)
+    for hop in range(1, peers):
+        current = lax.ppermute(current, axis, left)
+        so_far = so_far + product(current, (position + hop) % peers * rows)
+    return so_far
 
 
 def rms_scale(rows, gain):
@@ -138,11 +150,16 @@
     lifted = jnp.einsum("emd,edf->emf", arrived, expert_up, preferred_element_type=jnp.float32)
     activated = (jax.nn.silu(gate) * lifted).astype(jnp.bfloat16)
     out_width = expert_down.shape[2]
-    result = jnp.einsum(
-        "emf,efd->emd",
-        lax.all_gather(activated, "tp", axis=2, tiled=True),
-        expert_down,
-        preferred_element_type=jnp.float32,
+    result = ring_product(
+        activated,
+        "tp",
+        2,
+        lambda own_block, offset: jnp.einsum(
+            "emf,efd->emd",
+            own_block,
+            lax.dynamic_slice_in_dim(expert_down, offset, own_block.shape[2], axis=1),
+            preferred_element_type=jnp.float32,
+        ),
     ).astype(jnp.bfloat16)
     back = lax.all_to_all(
         result.reshape(local_experts, peers, capacity, out_width),

time: 169 us -> 188 us (1.11)
  starting transfers between devices: 6.62 us -> 28.6 us
  blocking collectives: 87.8 us -> 73.4 us
  waiting for transfers between devices: 32.8 us -> 42.2 us
    ppermute x0 -> x7, starting transfers between devices: none -> 22 us  [ring_product(): current = lax.ppermute(current, axis, left)]
    all_gather x1 -> x0, blocking collectives: 14.4 us -> none  [per_device(): lax.all_gather(activated, 'tp', axis=2, tiled=True)]
    ppermute x0 -> x7, waiting for transfers between devices: none -> 9.49 us  [ring_product(): current = lax.ppermute(current, axis, left)]
  transfers between devices with their start and end apart: 3 -> 10, of which waited for: 3 -> 10; matrix products, arithmetic and copies ran while one was open for 1% -> 2% of each run, Pallas kernels for 0% -> 0%
where the time goes in v1:
time: 188 us
  blocking collectives  73.4 us (39%)
  waiting for transfers between devices  42.2 us (22%)
  starting transfers between devices  28.6 us (15%)
  between operations  14.5 us (8%)
  matrix products  13.4 us (7%)
  other arithmetic  8.47 us (5%)
  local copies, waits for them, and re-layouts  6.99 us (4%)
    unnamed x2, waiting for transfers between devices  23.2 us
    ppermute x7, starting transfers between devices, ring_product(): current = lax.ppermute(current, axis, left)  22 us
    psum x1, blocking collectives, per_device(): squares = lax.psum(jnp.sum(after_float * after_float, axis=1), 'tp')  16.8 us
    all_gather x1, blocking collectives, per_device(): full_rows = lax.all_gather(hidden, 'tp', axis=1, tiled=True)  16.4 us
    all_gather x1, blocking collectives, per_device(): arrived = lax.all_gather(arrived, 'tp', axis=3, tiled=True)  15.5 us
    all_gather x1, blocking collectives, per_device(): lax.all_gather(mixed, 'tp', axis=1, tiled=True)  14.2 us
    all_to_all x1, blocking collectives, per_device(): lax.all_to_all(normed, 'ep', split_axis=1, concat_axis=0, tiled=True)  10.6 us
    ppermute x7, waiting for transfers between devices, ring_product(): current = lax.ppermute(current, axis, left)  9.49 us
  transfers between devices with their start and end apart: 10, of which 10 were waited for; matrix products, arithmetic and copies ran while one was open for 2% of the time, Pallas kernels for 0%

profile of v1, /device:TPU:0, one launch (start us, length us, event | category | flops | bytes accessed | tf_op | source)
XLA Modules:
  0.0 187.5 jit_solution(10967369341184386399)
XLA Ops:
  7.2 16.4 %all_gather.9 = bf16[40,4096]{1,0:T(8,128)(2,1)S(1)} all-gather(bf16[40,512]{1,0:T(8,128)(2,1)} %param.16), channel_id=1, replica_groups=mesh['ep'=4,'tp'=8] {'tp'}, dimensions={1}, use_global_device_ids=true | all-gather | bytes 368640 | tf_op jit(solution)/shard_map/all_gather | solution.py:94
  23.6 0.2 fusion.12
  23.8 0.9 fusion.14
  24.7 10.6 %all_to_all.42 = bf16[40,4,1024]{2,0,1:T(8,128)(2,1)S(1)} all-to-all(bf16[40,4,1024]{2,0,1:T(8,128)(2,1)S(1)} %bitcast.54), channel_id=1, replica_groups=mesh['ep'=4,'tp'=8] {'ep'}, dimensions={1} | all-to-all | bytes 655360 | tf_op jit(solution)/shard_map/all_to_all | solution.py:96
  35.3 2.9 %fusion = f32[160,1024]{1,0:T(8,128)} fusion(bf16[160,1024]{1,0:T(8,128)(2,1)S(1)} %bitcast.58, bf16[1024,256]{1,0:T(8,128)(2,1)} %param.22, bf16[1024,256]{1,0:T(8,128)(2,1)} %param.21, bf16[1024,256]{1,0:T(8,128)(2,1)} %param.20, bf16[1024,256]{1,0:T(8,128)(2,1)} %param.19), kind=kOutput, calls=%fused_computation.2 | convolution fusion | flops 343932928 | bytes 3080192 | tf_op jit(solution)/shard_map/dot_general | solution.py:100
  38.3 0.1 copy.65
  38.4 0.1 eq.40
  38.5 0.1 reshape.300
  38.7 0.1 reduce_window_sum.11
  38.8 0.2 select_reduce_fusion
  39.0 0.1 reduce_sum.71
  39.2 0.8 dynamic_slice.27
  40.1 0.2 multiply_cosine_fusion
  40.3 23.2 %reduce-scatter.4.cloned.1.call-done = f32[40,1024]{1,0:T(8,128)} async-done(((f32[160,1024]{1,0:T(8,128)}), f32[40,1024]{1,0:T(8,128)}) %reduce-scatter.4.cloned.1.call-update) | async-done | bytes 163856
  63.4 0.9 convert.10
  64.5 0.2 multiply_subtract_fusion
  64.7 0.2 pad_maximum_fusion
  64.9 4.1 %multiply_add_fusion = f32[40,2,128,128]{3,2,1,0:T(8,128)S(1)} fusion(f32[40,2,128,128]{3,2,1,0:T(8,128)} %param.18, f32[40,2,128]{2,1,0:T(2,128)S(1)} %reshape.305, f32[40,2,128]{2,1,0:T(2,128)S(1)} %get-tuple-element.16, f32[2]{0:T(128)S(1)} %log_exponential_fusion), kind=kLoop, calls=%fused_computation.1 | loop fusion | flops 3932160 | bytes 10567688 | tf_op jit(solution)/shard_map/add | solution.py:62
  69.0 2.3 %copy-done.1 = f32[40,2,128,128]{3,2,1,0:T(8,128)} copy-done((f32[40,2,128,128]{3,2,1,0:T(8,128)}, f32[40,2,128,128]{3,2,1,0:T(8,128)S(1)}, u32[]{:S(2)}) %copy-start.1) | copy-done | bytes 5242904
  71.3 4.5 %fusion.49 = f32[40,2,1,128]{3,2,1,0:T(1,128)S(1)} fusion(f32[40,2,128,1]{2,3,1,0:T(1,128)S(1)} %bitcast.61, f32[40,2,128,128]{3,2,1,0:T(8,128)S(1)} %multiply_add_fusion), kind=kOutput, calls=%fused_computation.102 | convolution fusion | flops 15728640 | bytes 5324800 | tf_op jit(solution)/shard_map/bhd,bhde->bhe/dot_general | solution.py:65
  75.8 0.1 reduce_sum.68
  76.0 0.2 multiply_reduce_fusion.2
  76.2 0.1 subtract_multiply_fusion
  76.4 14.2 %all_gather.10 = bf16[40,2048]{1,0:T(8,128)(2,1)S(1)} all-gather(bf16[40,256]{1,0:T(8,128)(2,1)S(1)} %fusion.34), channel_id=1, replica_groups=mesh['ep'=4,'tp'=8] {'tp'}, dimensions={1}, use_global_device_ids=true | all-gather | bytes 184320 | tf_op jit(solution)/shard_map/all_gather | solution.py:113
  90.5 0.6 multiply_reduce_fusion.1
  91.1 16.8 %psum.7 = f32[40]{0:T(128)S(1)} all-reduce(f32[40]{0:T(128)S(1)} %get-tuple-element.13), channel_id=1, replica_groups=mesh['ep'=4,'tp'=8] {'tp'}, use_global_device_ids=true, to_apply=%region_8.9 | all-reduce | flops 40 | bytes 320 | tf_op jit(solution)/shard_map/psum | solution.py:133
  107.9 0.2 convolution_convert_fusion
  108.2 0.7 copy.67
  108.9 3.3 %all-to-all-start.1 = ((bf16[4,2,10,512]{3,1,2,0:T(2,128)(2,1)}), bf16[4,2,10,512]{3,1,2,0:T(2,128)(2,1)S(1)}, u32[]{:S(2)}, u32[]{:S(2)}) async-start(bf16[4,2,10,512]{3,1,2,0:T(2,128)(2,1)} %copy.67), calls=%async_computation.1 | async-start | bytes 163840 | tf_op jit(solution)/shard_map/all_to_all | solution.py:140
  112.3 0.1 copy.72
  112.4 4.6 %all-to-all-done.1 = bf16[4,2,10,512]{3,1,2,0:T(2,128)(2,1)S(1)} async-done(((bf16[4,2,10,512]{3,1,2,0:T(2,128)(2,1)}), bf16[4,2,10,512]{3,1,2,0:T(2,128)(2,1)S(1)}, u32[]{:S(2)}, u32[]{:S(2)}) %all-to-all-start.1) | async-done | bytes 81952 | tf_op jit(solution)/shard_map/all_to_all | solution.py:140
  117.0 15.5 %all_gather.11 = bf16[1,2,40,4096]{3,2,1,0:T(8,128)(2,1)S(1)} all-gather(bf16[1,2,40,512]{3,2,1,0:T(8,128)(2,1)S(1)} %copy.68), channel_id=1, replica_groups=mesh['ep'=4,'tp'=8] {'tp'}, dimensions={3}, use_global_device_ids=true | all-gather | bytes 737280 | tf_op jit(solution)/shard_map/all_gather | solution.py:147
  132.5 2.9 %fusion.16 = f32[2,40,256]{2,1,0:T(8,128)S(1)} fusion(bf16[2,4096,256]{2,1,0:T(8,128)(2,1)} %param.27, bf16[1,2,40,4096]{3,2,1,0:T(8,128)(2,1)S(1)} %all_gather.11), kind=kOutput, calls=%fused_computation.30 | convolution fusion | flops 167772160 | bytes 4931584 | tf_op jit(solution)/shard_map/emd,edf->emf/dot_general | solution.py:149
  135.4 0.7 fusion.9
  136.1 0.7 collective-permute-start
  136.8 0.8 copy-done.2
  137.6 0.2 fusion.25
  137.8 0.7 collective-permute-done
  138.5 3.5 %collective-permute-start.1 = (bf16[2,40,256]{2,1,0:T(8,128)(2,1)S(1)}, bf16[2,40,256]{2,1,0:T(8,128)(2,1)S(1)}, u32[]{:S(2)}, u32[]{:S(2)}) collective-permute-start(bf16[2,40,256]{2,1,0:T(8,128)(2,1)S(1)} %collective-permute-done), channel_id=1, source_target_pairs={{0,7},{1,0},{2,1},{3,2},{4,3},{5,4},{6,5},{7,6},{8,15},{9,8},{10,9... | collective-permute-start | bytes 122888 | tf_op jit(solution)/shard_map/ppermute | solution.py:22
  142.0 0.2 convolution_add_fusion.6
  142.2 1.5 collective-permute-done.1
  143.7 3.5 %collective-permute-start.2 = (bf16[2,40,256]{2,1,0:T(8,128)(2,1)S(1)}, bf16[2,40,256]{2,1,0:T(8,128)(2,1)S(1)}, u32[]{:S(2)}, u32[]{:S(2)}) collective-permute-start(bf16[2,40,256]{2,1,0:T(8,128)(2,1)S(1)} %collective-permute-done.1), channel_id=1, source_target_pairs={{0,7},{1,0},{2,1},{3,2},{4,3},{5,4},{6,5},{7,6},{8,15},{9,8},{10,9... | collective-permute-start | bytes 122888 | tf_op jit(solution)/shard_map/ppermute | solution.py:22
  147.2 0.2 convolution_add_fusion.5
  147.4 1.5 collective-permute-done.2
  148.9 3.5 %collective-permute-start.3 = (bf16[2,40,256]{2,1,0:T(8,128)(2,1)S(1)}, bf16[2,40,256]{2,1,0:T(8,128)(2,1)S(1)}, u32[]{:S(2)}, u32[]{:S(2)}) collective-permute-start(bf16[2,40,256]{2,1,0:T(8,128)(2,1)S(1)} %collective-permute-done.2), channel_id=1, source_target_pairs={{0,7},{1,0},{2,1},{3,2},{4,3},{5,4},{6,5},{7,6},{8,15},{9,8},{10,9... | collective-permute-start | bytes 122888 | tf_op jit(solution)/shard_map/ppermute | solution.py:22
  152.5 0.2 convolution_add_fusion.4
  152.7 1.5 collective-permute-done.3
  154.1 3.5 %collective-permute-start.4 = (bf16[2,40,256]{2,1,0:T(8,128)(2,1)S(1)}, bf16[2,40,256]{2,1,0:T(8,128)(2,1)S(1)}, u32[]{:S(2)}, u32[]{:S(2)}) collective-permute-start(bf16[2,40,256]{2,1,0:T(8,128)(2,1)S(1)} %collective-permute-done.3), channel_id=1, source_target_pairs={{0,7},{1,0},{2,1},{3,2},{4,3},{5,4},{6,5},{7,6},{8,15},{9,8},{10,9... | collective-permute-start | bytes 122888 | tf_op jit(solution)/shard_map/ppermute | solution.py:22
  157.7 0.2 convolution_add_fusion.3
  157.9 1.5 collective-permute-done.4
  159.4 3.5 %collective-permute-start.5 = (bf16[2,40,256]{2,1,0:T(8,128)(2,1)S(1)}, bf16[2,40,256]{2,1,0:T(8,128)(2,1)S(1)}, u32[]{:S(2)}, u32[]{:S(2)}) collective-permute-start(bf16[2,40,256]{2,1,0:T(8,128)(2,1)S(1)} %collective-permute-done.4), channel_id=1, source_target_pairs={{0,7},{1,0},{2,1},{3,2},{4,3},{5,4},{6,5},{7,6},{8,15},{9,8},{10,9... | collective-permute-start | bytes 122888 | tf_op jit(solution)/shard_map/ppermute | solution.py:22
  162.9 0.2 convolution_add_fusion.2
  163.1 1.5 collective-permute-done.5
  164.6 3.5 %collective-permute-start.6 = (bf16[2,40,256]{2,1,0:T(8,128)(2,1)S(1)}, bf16[2,40,256]{2,1,0:T(8,128)(2,1)S(1)}, u32[]{:S(2)}, u32[]{:S(2)}) collective-permute-start(bf16[2,40,256]{2,1,0:T(8,128)(2,1)S(1)} %collective-permute-done.5), channel_id=1, source_target_pairs={{0,7},{1,0},{2,1},{3,2},{4,3},{5,4},{6,5},{7,6},{8,15},{9,8},{10,9... | collective-permute-start | bytes 122888 | tf_op jit(solution)/shard_map/ppermute | solution.py:22
  168.1 0.2 convolution_add_fusion.1
  168.3 1.5 collective-permute-done.6
  169.8 0.2 fusion.8
  170.0 0.7 copy.69
  170.7 3.3 %all-to-all-start.2 = ((bf16[2,4,10,512]{3,0,2,1:T(2,128)(2,1)}), bf16[2,4,10,512]{3,0,2,1:T(2,128)(2,1)S(1)}, u32[]{:S(2)}, u32[]{:S(2)}) async-start(bf16[2,4,10,512]{3,0,2,1:T(2,128)(2,1)} %bitcast.10), calls=%async_computation.2 | async-start | bytes 163840 | tf_op jit(solution)/shard_map/all_to_all | solution.py:164
  174.0 4.8 %all-to-all-done.2 = bf16[2,4,10,512]{3,0,2,1:T(2,128)(2,1)S(1)} async-done(((bf16[2,4,10,512]{3,0,2,1:T(2,128)(2,1)}), bf16[2,4,10,512]{3,0,2,1:T(2,128)(2,1)S(1)}, u32[]{:S(2)}, u32[]{:S(2)}) %all-to-all-start.2) | async-done | bytes 81952 | tf_op jit(solution)/shard_map/all_to_all | solution.py:164
  178.9 0.7 gather_fusion
  179.7 0.1 reshape.306
  179.8 0.3 multiply_reduce_fusion
  180.1 0.6 add_convert_fusion
  (41 shorter events, 0.7 us)
Async XLA Ops:
  7.2 83.4 %copy-start = (bf16[2048,512]{1,0:T(8,128)(2,1)S(1)}, bf16[2048,512]{1,0:T(8,128)(2,1)}, u32[]{:S(2)}) copy-start(bf16[2048,512]{1,0:T(8,128)(2,1)} %param.24) | copy-start | bytes 6291460
  7.2 56.3 %reduce-scatter.4.cloned.1.call-start = ((), (), s32[]{:S(2)}) async-start(), calls=%async_computation.4 | async-start | bytes 819200
  35.3 2.9 %copy-start.5 = (s32[40,2]{0,1:T(2,128)S(1)}, s32[40,2]{0,1:T(2,128)}, u32[]{:S(2)}) copy-start(s32[40,2]{0,1:T(2,128)} %param.30) | copy-start | bytes 964
  35.3 3.3 %copy-start.8 = (s32[40]{0:T(128)S(1)}, s32[40]{0:T(128)}, u32[]{:S(2)}) copy-start(s32[40]{0:T(128)} %param.17) | copy-start | bytes 484
  68.9 2.4 %copy-start.1 = (f32[40,2,128,128]{3,2,1,0:T(8,128)}, f32[40,2,128,128]{3,2,1,0:T(8,128)S(1)}, u32[]{:S(2)}) copy-start(f32[40,2,128,128]{3,2,1,0:T(8,128)S(1)} %multiply_add_fusion) | copy-start | bytes 15728644
  68.9 7.4 %copy-start.7 = (f32[256]{0:T(256)S(1)}, f32[256]{0:T(256)}, u32[]{:S(2)}) copy-start(f32[256]{0:T(256)} %param.23) | copy-start | bytes 3076
  68.9 21.6 %copy-start.4 = (bf16[40,512]{1,0:T(8,128)(2,1)S(1)}, bf16[40,512]{1,0:T(8,128)(2,1)}, u32[]{:S(2)}) copy-start(bf16[40,512]{1,0:T(8,128)(2,1)} %param.16) | copy-start | bytes 122884
  71.3 41.0 %copy-start.6 = (f32[40,2]{0,1:T(2,128)S(1)}, f32[40,2]{0,1:T(2,128)}, u32[]{:S(2)}) copy-start(f32[40,2]{0,1:T(2,128)} %param.31) | copy-start | bytes 964
  108.9 8.2 %all-to-all-start.1 = ((bf16[4,2,10,512]{3,1,2,0:T(2,128)(2,1)}), bf16[4,2,10,512]{3,1,2,0:T(2,128)(2,1)S(1)}, u32[]{:S(2)}, u32[]{:S(2)}) async-start(bf16[4,2,10,512]{3,1,2,0:T(2,128)(2,1)} %copy.67), calls=%async_computation.1 | async-start | bytes 163840 | tf_op jit(solution)/shard_map/all_to_all | solution.py:140
  117.0 18.4 %copy-start.3 = (bf16[2,4096,256]{2,1,0:T(8,128)(2,1)S(1)}, bf16[2,4096,256]{2,1,0:T(8,128)(2,1)}, u32[]{:S(2)}) copy-start(bf16[2,4096,256]{2,1,0:T(8,128)(2,1)} %param.28) | copy-start | bytes 12582916
  135.4 2.2 %copy-start.2 = (bf16[2,2048,512]{2,1,0:T(8,128)(2,1)S(1)}, bf16[2,2048,512]{2,1,0:T(8,128)(2,1)}, u32[]{:S(2)}) copy-start(bf16[2,2048,512]{2,1,0:T(8,128)(2,1)} %param.29) | copy-start | bytes 12582916
  136.1 2.3 %collective-permute-start = (bf16[2,40,256]{2,1,0:T(8,128)(2,1)S(1)}, bf16[2,40,256]{2,1,0:T(8,128)(2,1)S(1)}, u32[]{:S(2)}, u32[]{:S(2)}) collective-permute-start(bf16[2,40,256]{2,1,0:T(8,128)(2,1)S(1)} %fusion.9), channel_id=1, source_target_pairs={{0,7},{1,0},{2,1},{3,2},{4,3},{5,4},{6,5},{7,6},{8,15},{9,8},{10,9... | collective-permute-start | bytes 122888 | tf_op jit(solution)/shard_map/ppermute | solution.py:22
  138.5 5.2 %collective-permute-start.1 = (bf16[2,40,256]{2,1,0:T(8,128)(2,1)S(1)}, bf16[2,40,256]{2,1,0:T(8,128)(2,1)S(1)}, u32[]{:S(2)}, u32[]{:S(2)}) collective-permute-start(bf16[2,40,256]{2,1,0:T(8,128)(2,1)S(1)} %collective-permute-done), channel_id=1, source_target_pairs={{0,7},{1,0},{2,1},{3,2},{4,3},{5,4},{6,5},{7,6},{8,15},{9,8},{10,9... | collective-permute-start | bytes 122888 | tf_op jit(solution)/shard_map/ppermute | solution.py:22
  143.7 5.2 %collective-permute-start.2 = (bf16[2,40,256]{2,1,0:T(8,128)(2,1)S(1)}, bf16[2,40,256]{2,1,0:T(8,128)(2,1)S(1)}, u32[]{:S(2)}, u32[]{:S(2)}) collective-permute-start(bf16[2,40,256]{2,1,0:T(8,128)(2,1)S(1)} %collective-permute-done.1), channel_id=1, source_target_pairs={{0,7},{1,0},{2,1},{3,2},{4,3},{5,4},{6,5},{7,6},{8,15},{9,8},{10,9... | collective-permute-start | bytes 122888 | tf_op jit(solution)/shard_map/ppermute | solution.py:22
  148.9 5.2 %collective-permute-start.3 = (bf16[2,40,256]{2,1,0:T(8,128)(2,1)S(1)}, bf16[2,40,256]{2,1,0:T(8,128)(2,1)S(1)}, u32[]{:S(2)}, u32[]{:S(2)}) collective-permute-start(bf16[2,40,256]{2,1,0:T(8,128)(2,1)S(1)} %collective-permute-done.2), channel_id=1, source_target_pairs={{0,7},{1,0},{2,1},{3,2},{4,3},{5,4},{6,5},{7,6},{8,15},{9,8},{10,9... | collective-permute-start | bytes 122888 | tf_op jit(solution)/shard_map/ppermute | solution.py:22
  154.1 5.2 %collective-permute-start.4 = (bf16[2,40,256]{2,1,0:T(8,128)(2,1)S(1)}, bf16[2,40,256]{2,1,0:T(8,128)(2,1)S(1)}, u32[]{:S(2)}, u32[]{:S(2)}) collective-permute-start(bf16[2,40,256]{2,1,0:T(8,128)(2,1)S(1)} %collective-permute-done.3), channel_id=1, source_target_pairs={{0,7},{1,0},{2,1},{3,2},{4,3},{5,4},{6,5},{7,6},{8,15},{9,8},{10,9... | collective-permute-start | bytes 122888 | tf_op jit(solution)/shard_map/ppermute | solution.py:22
  159.4 5.2 %collective-permute-start.5 = (bf16[2,40,256]{2,1,0:T(8,128)(2,1)S(1)}, bf16[2,40,256]{2,1,0:T(8,128)(2,1)S(1)}, u32[]{:S(2)}, u32[]{:S(2)}) collective-permute-start(bf16[2,40,256]{2,1,0:T(8,128)(2,1)S(1)} %collective-permute-done.4), channel_id=1, source_target_pairs={{0,7},{1,0},{2,1},{3,2},{4,3},{5,4},{6,5},{7,6},{8,15},{9,8},{10,9... | collective-permute-start | bytes 122888 | tf_op jit(solution)/shard_map/ppermute | solution.py:22
  164.6 5.2 %collective-permute-start.6 = (bf16[2,40,256]{2,1,0:T(8,128)(2,1)S(1)}, bf16[2,40,256]{2,1,0:T(8,128)(2,1)S(1)}, u32[]{:S(2)}, u32[]{:S(2)}) collective-permute-start(bf16[2,40,256]{2,1,0:T(8,128)(2,1)S(1)} %collective-permute-done.5), channel_id=1, source_target_pairs={{0,7},{1,0},{2,1},{3,2},{4,3},{5,4},{6,5},{7,6},{8,15},{9,8},{10,9... | collective-permute-start | bytes 122888 | tf_op jit(solution)/shard_map/ppermute | solution.py:22
  170.7 8.2 %all-to-all-start.2 = ((bf16[2,4,10,512]{3,0,2,1:T(2,128)(2,1)}), bf16[2,4,10,512]{3,0,2,1:T(2,128)(2,1)S(1)}, u32[]{:S(2)}, u32[]{:S(2)}) async-start(bf16[2,4,10,512]{3,0,2,1:T(2,128)(2,1)} %bitcast.10), calls=%async_computation.2 | async-start | bytes 163840 | tf_op jit(solution)/shard_map/all_to_all | solution.py:164
Sparse Core Ops, SparseCore 0:
  38.4 25.0 reduce-scatter.3
